TPU v7x, 32 devices: a whole 2x2x4 slice. The times are simulated.
32 devices in a mesh: ep: 16 (over z, y, core), tp: 2 (over x).
Axes of the slice: x: 2, y: 2, z: 4, core: 2. Of those that a mesh axis runs over, the one named last changes fastest.
Arguments:
- tokens: bfloat16 [2048, 2048], P('ep'), may hold values from -6 to 6
- expert_ids: int32 [2048, 2], P('ep'), may hold values from 0 to 15, as said below
- route_weights: bfloat16 [2048, 2], P('ep'), may hold values from 0.099609375 to 1
- cotangent: bfloat16 [2048, 2048], P('ep'), may hold values from -3 to 3
- w_gate: bfloat16 [16, 2048, 512], P('ep', None, 'tp'), may hold values from -0.125 to 0.125
- w_up: bfloat16 [16, 2048, 512], P('ep', None, 'tp'), may hold values from -0.125 to 0.125
- w_down: bfloat16 [16, 512, 2048], P('ep', 'tp'), may hold values from -0.25 to 0.25
Outputs:
- token_grad: bfloat16 [2048, 2048], P('ep', 'tp')
- route_grad: bfloat16 [2048, 2], P('ep')
- grad_gate: bfloat16 [16, 2048, 512], P('ep', None, 'tp')
- grad_up: bfloat16 [16, 2048, 512], P('ep', None, 'tp')
- grad_down: bfloat16 [16, 512, 2048], P('ep', 'tp')
- gate_rows: float32 [16, 2048], P('ep')
- up_rows: float32 [16, 2048], P('ep')
- down_rows: float32 [16, 512], P('ep', 'tp')
Inputs may be any that keep to these rules, and one draw needn't show every extreme that they name: `expert_ids`: each row names 2 different experts of one group: both lie in g * 4 to (g + 1) * 4 - 1 for the row's group g. In the rows of one device (aligned blocks of 128 rows) no expert is named more than 32 times, and in every block some expert is named exactly 32 times.
All inputs are finite; a program needn't handle non-finite values.
Results may differ from a plain program's by a relative error of at most 0.012.
Values may be sent and summed in bfloat16 or wider, within the bound.
A program may use at most 64 MiB of HBM per device.

v0:
```python
import jax
import jax.numpy as jnp
from jax import lax
from jax.sharding import PartitionSpec as P

TOPK = 2


def on_device(tokens, expert_ids, route_weights, cotangent, w_gate, w_up, w_down):
    tok_rows, model_width = tokens.shape
    experts = lax.axis_size("ep")
    splits = lax.axis_size("tp")
    capacity = 2 * tok_rows * TOPK // experts
    slot_count = experts * capacity
    assigns = tok_rows * TOPK
    flat_ids = expert_ids.reshape(-1)
    onehot = (flat_ids[:, None] == jnp.arange(experts, dtype=jnp.int32)[None, :]).astype(
        jnp.float32
    )
    assign_order = jnp.arange(assigns, dtype=jnp.int32)
    earlier = (assign_order[:, None] > assign_order[None, :]).astype(jnp.float32)
    before = jnp.dot(earlier, onehot, precision=lax.Precision.HIGHEST)
    slot_rank = jnp.sum(before * onehot, axis=1).astype(jnp.int32)
    position = flat_ids * capacity + slot_rank
    slot_owner = jnp.full((slot_count,), tok_rows, jnp.int32).at[position].set(assign_order // TOPK)
    slot_scale = jnp.zeros((slot_count,), jnp.bfloat16).at[position].set(route_weights.reshape(-1))
    slice_width = model_width // splits
    slice_start = lax.axis_index("tp") * slice_width
    rows_slice = lax.dynamic_slice_in_dim(tokens, slice_start, slice_width, 1)
    cot_slice = lax.dynamic_slice_in_dim(cotangent, slice_start, slice_width, 1)
    rows_pad = jnp.concatenate([rows_slice, jnp.zeros((1, slice_width), jnp.bfloat16)], axis=0)
    cot_pad = jnp.concatenate([cot_slice, jnp.zeros((1, slice_width), jnp.bfloat16)], axis=0)
    outgoing = rows_pad[slot_owner]
    outgoing_cot = cot_pad[slot_owner]
    part_rows, part_cot, got_scale = (
        lax.all_to_all(outgoing, "ep", split_axis=0, concat_axis=0, tiled=True),
        lax.all_to_all(outgoing_cot, "ep", split_axis=0, concat_axis=0, tiled=True),
        lax.all_to_all(slot_scale, "ep", split_axis=0, concat_axis=0, tiled=True),
    )
    slot_rows, slot_cot = (
        lax.all_gather(part_rows, "tp", axis=1, tiled=True),
        lax.all_gather(part_cot, "tp", axis=1, tiled=True),
    )
    scale_col = got_scale.reshape(slot_count, 1).astype(jnp.float32)
    gate_cols = w_gate[0]
    up_cols = w_up[0]
    down_part = w_down[0]
    gate_pre = jnp.dot(slot_rows, gate_cols, preferred_element_type=jnp.float32)
    up_pre = jnp.dot(slot_rows, up_cols, preferred_element_type=jnp.float32)
    hidden_back = lax.dot_general(
        slot_cot, down_part, (((1,), (1,)), ((), ())), preferred_element_type=jnp.float32
    )
    gate_sig = jax.nn.sigmoid(gate_pre)
    activated = gate_pre * gate_sig
    hidden = activated * up_pre
    route_part = jnp.sum(hidden * hidden_back, axis=1)
    hidden_cot = scale_col * hidden_back
    up_cot = (hidden_cot * activated).astype(jnp.bfloat16)
    gate_cot = (hidden_cot * up_pre * gate_sig * (1.0 + gate_pre * (1.0 - gate_sig))).astype(
        jnp.bfloat16
    )
    weighted_hidden = (scale_col * hidden).astype(jnp.bfloat16)
    grad_down = lax.dot_general(
        weighted_hidden, slot_cot, (((0,), (0,)), ((), ())), preferred_element_type=jnp.float32
    ).astype(jnp.bfloat16)
    grad_gate = lax.dot_general(
        slot_rows, gate_cot, (((0,), (0,)), ((), ())), preferred_element_type=jnp.float32
    ).astype(jnp.bfloat16)
    grad_up = lax.dot_general(
        slot_rows, up_cot, (((0,), (0,)), ((), ())), preferred_element_type=jnp.float32
    ).astype(jnp.bfloat16)
    token_term = lax.dot_general(
        gate_cot, gate_cols, (((1,), (1,)), ((), ())), preferred_element_type=jnp.float32
    )
    token_term = token_term + lax.dot_general(
        up_cot, up_cols, (((1,), (1,)), ((), ())), preferred_element_type=jnp.float32
    )
    reduced = lax.psum_scatter(
        token_term.astype(jnp.bfloat16), "tp", scatter_dimension=1, tiled=True
    )
    gate_square = jnp.sum(jnp.square(grad_gate.astype(jnp.float32)), axis=1)
    up_square = jnp.sum(jnp.square(grad_up.astype(jnp.float32)), axis=1)
    down_square = jnp.sum(jnp.square(grad_down.astype(jnp.float32)), axis=1)
    route_total, gate_rows, up_rows = lax.psum((route_part, gate_square, up_square), "tp")
    back_rows, back_route = (
        lax.all_to_all(reduced, "ep", split_axis=0, concat_axis=0, tiled=True),
        lax.all_to_all(
            route_total.astype(jnp.bfloat16), "ep", split_axis=0, concat_axis=0, tiled=True
        ),
    )
    per_assign = back_rows[position].astype(jnp.float32).reshape(tok_rows, TOPK, -1)
    token_grad = jnp.sum(per_assign, axis=1).astype(jnp.bfloat16)
    route_grad = back_route[position].reshape(tok_rows, TOPK)
    return (
        token_grad,
        route_grad,
        grad_gate[None],
        grad_up[None],
        grad_down[None],
        gate_rows[None],
        up_rows[None],
        down_square[None],
    )


def solution(mesh):
    return jax.shard_map(
        on_device,
        mesh=mesh,
        in_specs=(
            P("ep", None),
            P("ep", None),
            P("ep", None),
            P("ep", None),
            P("ep", None, "tp"),
            P("ep", None, "tp"),
            P("ep", "tp", None),
        ),
        out_specs=(
            P("ep", "tp"),
            P("ep", None),
            P("ep", None, "tp"),
            P("ep", None, "tp"),
            P("ep", "tp", None),
            P("ep", None),
            P("ep", None),
            P("ep", "tp"),
        ),
        check_vma=False,
    )
```

profile of v0, /device:TPU:9, one launch (start us, length us, event | category | flops | bytes accessed | tf_op | source)
XLA Modules:
  0.0 192.4 jit_solution(12211207150902373876)
XLA Ops:
  7.2 0.0 copy-start
  7.2 0.0 all-gather.5.cloned.1.call-start
  7.2 0.8 broadcast_multiply_fusion
  8.0 0.8 copy.24
  8.8 0.1 copy.23
  8.9 0.1 mul.62
  9.0 0.1 eq.15
  9.2 0.2 fusion
  9.4 1.4 scatter_custom_fusion.1
  10.8 1.1 constant_dynamic-slice_fusion
  11.9 2.1 %gather_fusion.1 = bf16[512,1024]{1,0:T(8,128)(2,1)S(1)} fusion(bf16[129,1024]{1,0:T(8,128)(2,1)S(1)} %concatenate.7, s32[1024]{0:T(1024)S(1)} %pad_clamp_fusion.1), kind=kCustom, calls=%fused_computation.1 | custom fusion | bytes 2099200 | tf_op jit(solution)/shard_map/gather | solution.py:33
  14.0 31.8 %all_to_all.59 = bf16[16,32,1024]{2,1,0:T(8,128)(2,1)} all-to-all(bf16[16,32,1024]{2,1,0:T(8,128)(2,1)S(1)} %bitcast.43), channel_id=1, replica_groups=mesh['ep'=16,'tp'=2] {'ep'}, dimensions={0} | all-to-all | bytes 2097152 | tf_op jit(solution)/shard_map/all_to_all | solution.py:36
  45.8 0.0 all-gather.5.cloned.1.call-update
  45.9 0.0 all-gather.3.cloned.1.call-start
  45.9 2.1 %gather_fusion = bf16[512,1024]{1,0:T(8,128)(2,1)S(1)} fusion(bf16[129,1024]{1,0:T(8,128)(2,1)S(1)} %concatenate.6, s32[1024]{0:T(1024)S(1)} %pad_clamp_fusion.1), kind=kCustom, calls=%fused_computation | custom fusion | bytes 2099200 | tf_op jit(solution)/shard_map/gather | solution.py:34
  48.0 0.0 copy-start.2
  48.0 29.6 %all_to_all.60 = bf16[16,32,1024]{2,1,0:T(8,128)(2,1)} all-to-all(bf16[16,32,1024]{2,1,0:T(8,128)(2,1)S(1)} %bitcast.42), channel_id=1, replica_groups=mesh['ep'=16,'tp'=2] {'ep'}, dimensions={0} | all-to-all | bytes 2097152 | tf_op jit(solution)/shard_map/all_to_all | solution.py:37
  77.6 0.0 all-gather.3.cloned.1.call-update
  77.7 0.0 copy-start.1
  77.7 0.0 reduce-scatter.2.cloned.1.call-start
  77.7 0.0 copy-done.2
  77.7 0.1 copy.25
  77.9 0.1 reshape.116
  78.0 2.2 %scatter_custom_fusion = bf16[512]{0:T(512)(128)(2,1)S(1)} fusion(s32[256]{0:T(256)S(1)} %bitcast.52, bf16[256]{0:T(256)(128)(2,1)S(1)} %reshape.116, bf16[]{:T(256)} %constant.13.clone.1), kind=kCustom, calls=%fused_computation.49 | custom fusion | bytes 1026 | tf_op jit(solution)/shard_map/scatter | solution.py:26
  80.2 0.1 all_to_all.52
  80.3 8.9 %all_to_all.61 = bf16[16,32,1]{1,2,0:T(2,128)(2,1)S(1)} all-to-all(bf16[16,32,1]{1,2,0:T(2,128)(2,1)S(1)} %all_to_all.52), channel_id=1, replica_groups=mesh['ep'=16,'tp'=2] {'ep'}, dimensions={0} | all-to-all | bytes 2048 | tf_op jit(solution)/shard_map/all_to_all | solution.py:38
  89.2 0.1 reshape.79
  89.3 0.0 all-gather.5.cloned.1.call-done
  89.3 0.0 copy-done
  89.3 0.0 copy-start.3
  89.3 2.6 %fusion.3 = f32[512,256]{0,1:T(8,128)S(1)} fusion(bf16[512,2048]{1,0:T(8,128)(2,1)} %all-gather.5.cloned.1.call-done, bf16[1,2048,256]{2,1,0:T(8,128)(2,1)S(1)} %copy-done), kind=kOutput, calls=%fused_computation.17 | convolution fusion | flops 536870912 | bytes 3670016 | tf_op jit(solution)/shard_map/dot_general | solution.py:48
  91.9 0.0 copy-done.1
  91.9 0.0 copy-done.3
  91.9 0.0 copy-start.5
  91.9 1.6 fusion.6
  93.5 19.1 %all-gather.3.cloned.1.call-done = bf16[512,2048]{1,0:T(8,128)(2,1)} async-done(((bf16[512,1024]{1,0:T(8,128)(2,1)}), bf16[512,2048]{1,0:T(8,128)(2,1)}) %all-gather.3.cloned.1.call-update) | async-done | bytes 2097168 | tf_op jit(solution)/shard_map/all_gather | solution.py:42
  112.6 2.9 %multiply_reduce_fusion.3 = (f32[512]{0:T(512)S(1)}, bf16[512,256]{0,1:T(8,128)(2,1)S(1)}, bf16[512,256]{0,1:T(8,128)(2,1)S(1)}) fusion(f32[512,256]{0,1:T(8,128)} %fusion.6, f32[512,256]{0,1:T(8,128)S(1)} %fusion.3, f32[512]{0:T(512)S(1)} %reshape.79, bf16[512,2048]{1,0:T(8,128)(2,1)} %all-gather.3.cloned.1.call-done, bf16[1,256,2048]{2,1,0:T(8,128)(2,1)} %param.13), kind=kOutput, calls=%fused_computation.25 | convolution fusion | flops 539098624 | bytes 4722688 | tf_op jit(solution)/shard_map/dot_general | solution.py:50
  115.5 0.0 copy-done.5
  115.6 0.8 fusion.1
  116.3 2.1 %add_convert_fusion = bf16[512,2048]{1,0:T(8,128)(2,1)} fusion(f32[512,2048]{1,0:T(8,128)S(1)} %fusion.1, bf16[512,256]{0,1:T(8,128)(2,1)S(1)} %get-tuple-element.37, bf16[1,2048,256]{2,1,0:T(8,128)(2,1)S(1)} %copy-done.1), kind=kOutput, calls=%fused_computation.6 | convolution fusion | flops 538968064 | bytes 7602176 | tf_op jit(solution)/shard_map/dot_general | solution.py:75
  118.5 0.0 reduce-scatter.2.cloned.1.call-update
  118.5 0.0 copy-start.4
  118.5 2.5 %multiply_reduce_fusion.2 = (f32[2048]{0:T(1024)S(1)}, bf16[2048,256]{0,1:T(8,128)(2,1)S(1)}) fusion(bf16[512,256]{0,1:T(8,128)(2,1)S(1)} %get-tuple-element.36, bf16[512,2048]{1,0:T(8,128)(2,1)} %all-gather.5.cloned.1.call-done), kind=kOutput, calls=%fused_computation.12 | convolution fusion | flops 538966016 | bytes 3416064 | tf_op jit(solution)/shard_map/dot_general | solution.py:66
  121.0 0.0 copy-done.4
  121.0 1.7 multiply_reduce_fusion.1
  122.7 6.5 %all-reduce.2 = (bf16[512]{0:T(512)(128)(2,1)S(1)}, f32[1,2048]{1,0:T(1,128)}, f32[1,2048]{1,0:T(1,128)}) all-reduce(f32[512]{0:T(512)S(1)} %get-tuple-element.35, f32[1,2048]{1,0:T(1,128)S(1)} %bitcast.49, f32[1,2048]{1,0:T(1,128)S(1)} %bitcast.50), channel_id=1, replica_groups=mesh['ep'=16,'tp'=2] {'tp'}, use_global_device_ids=true, to_apply=%region_6.7 | all-reduce | flops 4608 | bytes 35840 | tf_op jit(solution)/shard_map/psum | solution.py:84
  129.2 0.1 all_to_all.53
  129.3 13.0 %all_to_all.62 = bf16[16,32,1]{1,2,0:T(2,128)(2,1)S(1)} all-to-all(bf16[16,32,1]{1,2,0:T(2,128)(2,1)S(1)} %all_to_all.53), channel_id=1, replica_groups=mesh['ep'=16,'tp'=2] {'ep'}, dimensions={0} | all-to-all | bytes 2048 | tf_op jit(solution)/shard_map/all_to_all | solution.py:87
  142.3 8.7 %reduce-scatter.2.cloned.1.call-done = bf16[512,1024]{1,0:T(8,128)(2,1)} async-done(((bf16[512,2048]{1,0:T(8,128)(2,1)}), bf16[512,1024]{1,0:T(8,128)(2,1)}) %reduce-scatter.2.cloned.1.call-update) | async-done | bytes 1048592 | tf_op jit(solution)/shard_map/reduce_scatter | solution.py:78
  150.9 6.5 %all-to-all-start.3 = ((bf16[16,32,1024]{2,1,0:T(8,128)(2,1)}), bf16[16,32,1024]{2,1,0:T(8,128)(2,1)S(1)}, u32[]{:S(2)}, u32[]{:S(2)}) async-start(bf16[16,32,1024]{2,1,0:T(8,128)(2,1)} %bitcast.46), calls=%async_computation.4 | async-start | bytes 2097152 | tf_op jit(solution)/shard_map/all_to_all | solution.py:86
  157.5 2.3 %copy.30 = bf16[1,2048,256]{2,1,0:T(8,128)(2,1)} copy(bf16[1,2048,256]{1,2,0:T(8,128)(2,1)} %bitcast.48) | data formatting | bytes 2097152
  159.7 1.3 copy.29
  161.0 4.2 %multiply_reduce_fusion = (f32[256]{0:T(256)}, bf16[256,2048]{1,0:T(8,128)(2,1)}) fusion(bf16[512,2048]{1,0:T(8,128)(2,1)} %all-gather.3.cloned.1.call-done, f32[512]{0:T(512)S(1)} %reshape.79, f32[512,256]{0,1:T(8,128)} %fusion.6, f32[512,256]{0,1:T(8,128)} %copy-done.5), kind=kOutput, calls=%fused_computation.10 | convolution fusion | flops 539885312 | bytes 4197376 | tf_op jit(solution)/shard_map/dot_general | solution.py:63
  165.3 0.1 all_to_all.51
  165.4 1.9 %gather_fusion.3 = bf16[256]{0:T(256)(128)(2,1)S(1)} fusion(bf16[512]{0:T(512)(128)(2,1)S(1)} %all_to_all.51, s32[1024]{0:T(1024)S(1)} %pad_clamp_fusion), kind=kCustom, calls=%fused_computation.3 | custom fusion | bytes 2048 | tf_op jit(solution)/shard_map/gather | solution.py:93
  167.3 0.2 reshape.78
  167.4 0.6 copy.28
  168.1 14.3 %all-to-all-done.3 = bf16[16,32,1024]{2,1,0:T(8,128)(2,1)S(1)} async-done(((bf16[16,32,1024]{2,1,0:T(8,128)(2,1)}), bf16[16,32,1024]{2,1,0:T(8,128)(2,1)S(1)}, u32[]{:S(2)}, u32[]{:S(2)}) %all-to-all-start.3) | async-done | bytes 1048608 | tf_op jit(solution)/shard_map/all_to_all | solution.py:86
  182.4 1.2 gather_fusion.2
  183.5 0.2 gather.17
  183.7 2.1 %reduce_sum.58 = bf16[128,1024]{1,0:T(8,128)(2,1)} reduce(bf16[128,2,1024]{2,1,0:T(2,128)(2,1)S(1)} %gather.17, bf16[]{:T(256)} %constant.13.clone.1), dimensions={1}, to_apply=%region_4.5 | reduce | flops 131072 | bytes 786434 | tf_op jit(solution)/shard_map/reduce_sum | solution.py:92
  (10 shorter events, 0.1 us)
Async XLA Ops:
  7.2 82.1 %copy-start = (bf16[1,2048,256]{2,1,0:T(8,128)(2,1)S(1)}, bf16[1,2048,256]{2,1,0:T(8,128)(2,1)}, u32[]{:S(2)}) copy-start(bf16[1,2048,256]{2,1,0:T(8,128)(2,1)} %param.11) | copy-start | bytes 3145732
  7.2 82.1 %all-gather.5.cloned.1.call-start = ((), (), s32[]{:S(2)}) async-start(), calls=%async_computation.7 | async-start | bytes 3145728 | tf_op jit(solution)/shard_map/all_gather | solution.py:41
  45.9 66.7 %all-gather.3.cloned.1.call-start = ((), (), s32[]{:S(2)}) async-start(), calls=%async_computation.6 | async-start | bytes 3145728 | tf_op jit(solution)/shard_map/all_gather | solution.py:42
  48.0 29.7 %copy-start.2 = (bf16[128,2]{0,1:T(2,128)(2,1)S(1)}, bf16[128,2]{0,1:T(2,128)(2,1)}, u32[]{:S(2)}) copy-start(bf16[128,2]{0,1:T(2,128)(2,1)} %param.9) | copy-start | bytes 1540
  77.7 14.2 %copy-start.1 = (bf16[1,2048,256]{2,1,0:T(8,128)(2,1)S(1)}, bf16[1,2048,256]{2,1,0:T(8,128)(2,1)}, u32[]{:S(2)}) copy-start(bf16[1,2048,256]{2,1,0:T(8,128)(2,1)} %param.12) | copy-start | bytes 3145732
  77.7 73.3 %reduce-scatter.2.cloned.1.call-start = ((), (), s32[]{:S(2)}) async-start(), calls=%async_computation.8 | async-start | bytes 3145728 | tf_op jit(solution)/shard_map/reduce_scatter | solution.py:78
  89.3 2.6 %copy-start.3 = (bf16[512,2048]{1,0:T(8,128)(2,1)S(1)}, bf16[512,2048]{1,0:T(8,128)(2,1)}, u32[]{:S(2)}) copy-start(bf16[512,2048]{1,0:T(8,128)(2,1)} %all-gather.5.cloned.1.call-done) | copy-start | bytes 6291460
  91.9 23.6 %copy-start.5 = (f32[512,256]{0,1:T(8,128)}, f32[512,256]{0,1:T(8,128)S(1)}, u32[]{:S(2)}) copy-start(f32[512,256]{0,1:T(8,128)S(1)} %fusion.3) | copy-start | bytes 1572868
  118.5 2.5 %copy-start.4 = (bf16[512,2048]{1,0:T(8,128)(2,1)S(1)}, bf16[512,2048]{1,0:T(8,128)(2,1)}, u32[]{:S(2)}) copy-start(bf16[512,2048]{1,0:T(8,128)(2,1)} %all-gather.5.cloned.1.call-done) | copy-start | bytes 6291460
  150.9 31.4 %all-to-all-start.3 = ((bf16[16,32,1024]{2,1,0:T(8,128)(2,1)}), bf16[16,32,1024]{2,1,0:T(8,128)(2,1)S(1)}, u32[]{:S(2)}, u32[]{:S(2)}) async-start(bf16[16,32,1024]{2,1,0:T(8,128)(2,1)} %bitcast.46), calls=%async_computation.4 | async-start | bytes 2097152 | tf_op jit(solution)/shard_map/all_to_all | solution.py:86
Sparse Core Ops, SparseCore 0:
  46.0 31.9 all-gather.4
  79.5 33.0 all-gather.2
  118.6 32.2 reduce-scatter.1
where the time goes:
time: 193 us; the launch traced here: 192 us
  blocking collectives  89.8 us (47%)
  waiting for transfers between devices  42.1 us (22%)
  matrix products  18.6 us (10%)
  local copies, waits for them, and re-layouts  18.2 us (9%)
  between operations  14 us (7%)
  starting transfers between devices  6.63 us (3%)
  other arithmetic  3 us (2%)
    all_to_all x1, blocking collectives, on_device(): lax.all_to_all(outgoing, 'ep', split_axis=0, concat_axis=0, tiled=True)  31.8 us
    all_to_all x1, blocking collectives, on_device(): lax.all_to_all(outgoing_cot, 'ep', split_axis=0, concat_axis=0, tiled=True)  29.6 us
    all_gather x1, waiting for transfers between devices, on_device(): lax.all_gather(part_cot, 'tp', axis=1, tiled=True)  19.1 us
    all_to_all x1, waiting for transfers between devices, on_device(): lax.all_to_all(reduced, 'ep', split_axis=0, concat_axis=0, tiled=True)  14.3 us
    all_to_all x1, blocking collectives, on_device(): lax.all_to_all(route_total.astype(jnp.bfloat16), 'ep', split_axis=0, conc...  13 us
    all_to_all x1, blocking collectives, on_device(): lax.all_to_all(slot_scale, 'ep', split_axis=0, concat_axis=0, tiled=True)  8.9 us
    reduce_scatter x1, waiting for transfers between devices, on_device(): lax.psum_scatter(token_term.astype(jnp.bfloat16), 'tp', scatter_dimension...  8.67 us
    psum x1, blocking collectives, on_device(): lax.psum((route_part, gate_square, up_square), 'tp')  6.52 us
  transfers between devices with their start and end apart: 4, of which 3 were waited for; matrix products, arithmetic and copies ran while one was open for 12% of the time, Pallas kernels for 0%

commit v1 on v0

--- a/solution.py
+++ b/solution.py
@@ -2,6 +2,7 @@
 import jax.numpy as jnp
 from jax import lax
 from jax.sharding import PartitionSpec as P
+from jax.lax import all_gather
 
 TOPK = 2
 
@@ -39,7 +40,7 @@
     )
     slot_rows, slot_cot = (
         lax.all_gather(part_rows, "tp", axis=1, tiled=True),
-        lax.all_gather(part_cot, "tp", axis=1, tiled=True),
+        jnp.concatenate(all_gather(part_cot, "tp"), 1),
     )
     scale_col = got_scale.reshape(slot_count, 1).astype(jnp.float32)
     gate_cols = w_gate[0]

time: 193 us -> 195 us (1.010)
  local copies, waits for them, and re-layouts: 18.2 us -> 21.8 us
  matrix products: 18.6 us -> 15.6 us
    all_gather x1, waiting for transfers between devices: 0.01 us -> 20.4 us  [on_device(): lax.all_gather(part_rows, 'tp', axis=1, tiled=True)]
    all_gather x1, waiting for transfers between devices: 19.1 us -> 0.01 us  [on_device(): all_gather(part_cot, 'tp')]
    all_gather x0 -> x1, local copies, waits for them, and re-layouts: none -> 2.93 us  [on_device(): all_gather(part_cot, 'tp')]
    all_to_all x1, blocking collectives: 29.6 us -> 31.8 us  [on_device(): lax.all_to_all(outgoing_cot, 'ep', split_axis=0, concat_axis=0, tiled=True)]
    all_to_all x1, blocking collectives: 31.8 us -> 29.6 us  [on_device(): lax.all_to_all(outgoing, 'ep', split_axis=0, concat_axis=0, tiled=True)]
    dot_general x1, matrix products: 2.94 us -> 0.92 us  [on_device(): lax.dot_general(slot_cot, down_part, (((1,), (1,)), ((), ())), preferred_...]
    unnamed x17 -> x27, local copies, waits for them, and re-layouts: 5.12 us -> 5.8 us
  transfers between devices with their start and end apart: 4 -> 4, of which waited for: 3 -> 3; matrix products, arithmetic and copies ran while one was open for 12% -> 11% of each run, Pallas kernels for 0% -> 0%
where the time goes in v1:
time: 195 us; the launch traced here: 194 us
  blocking collectives  89.8 us (46%)
  waiting for transfers between devices  43.4 us (22%)
  local copies, waits for them, and re-layouts  21.8 us (11%)
  matrix products  15.6 us (8%)
  between operations  14 us (7%)
  starting transfers between devices  6.63 us (3%)
  other arithmetic  2.94 us (2%)
    all_to_all x1, blocking collectives, on_device(): lax.all_to_all(outgoing_cot, 'ep', split_axis=0, concat_axis=0, tiled=True)  31.8 us
    all_to_all x1, blocking collectives, on_device(): lax.all_to_all(outgoing, 'ep', split_axis=0, concat_axis=0, tiled=True)  29.6 us
    all_gather x1, waiting for transfers between devices, on_device(): lax.all_gather(part_rows, 'tp', axis=1, tiled=True)  20.4 us
    all_to_all x1, waiting for transfers between devices, on_device(): lax.all_to_all(reduced, 'ep', split_axis=0, concat_axis=0, tiled=True)  14.3 us
    all_to_all x1, blocking collectives, on_device(): lax.all_to_all(route_total.astype(jnp.bfloat16), 'ep', split_axis=0, conc...  13 us
    all_to_all x1, blocking collectives, on_device(): lax.all_to_all(slot_scale, 'ep', split_axis=0, concat_axis=0, tiled=True)  8.9 us
    reduce_scatter x1, waiting for transfers between devices, on_device(): lax.psum_scatter(token_term.astype(jnp.bfloat16), 'tp', scatter_dimension...  8.68 us
    psum x1, blocking collectives, on_device(): lax.psum((route_part, gate_square, up_square), 'tp')  6.52 us
  transfers between devices with their start and end apart: 4, of which 3 were waited for; matrix products, arithmetic and copies ran while one was open for 11% of the time, Pallas kernels for 0%

profile of v1, /device:TPU:9, one launch (start us, length us, event | category | flops | bytes accessed | tf_op | source)
XLA Modules:
  0.0 194.3 jit_solution(3963568631655132502)
XLA Ops:
  7.2 0.0 copy-start
  7.2 0.0 all-gather.3.cloned.1.call-start
  7.2 0.8 broadcast_multiply_fusion
  8.0 0.8 copy.32
  8.8 0.1 copy.31
  8.9 0.1 mul.62
  9.0 0.1 eq.15
  9.2 0.2 fusion
  9.4 1.4 scatter_custom_fusion.1
  10.8 1.1 constant_dynamic-slice_fusion
  11.9 2.1 %gather_fusion = bf16[512,1024]{1,0:T(8,128)(2,1)S(1)} fusion(bf16[129,1024]{1,0:T(8,128)(2,1)S(1)} %concatenate.6, s32[1024]{0:T(1024)S(1)} %pad_clamp_fusion.1), kind=kCustom, calls=%fused_computation | custom fusion | bytes 2099200 | tf_op jit(solution)/shard_map/gather | solution.py:35
  14.0 31.8 %all_to_all.56 = bf16[16,32,1024]{2,1,0:T(8,128)(2,1)} all-to-all(bf16[16,32,1024]{2,1,0:T(8,128)(2,1)S(1)} %bitcast.46), channel_id=1, replica_groups=mesh['ep'=16,'tp'=2] {'ep'}, dimensions={0} | all-to-all | bytes 2097152 | tf_op jit(solution)/shard_map/all_to_all | solution.py:38
  45.8 0.0 all-gather.3.cloned.1.call-update
  45.9 0.0 all-gather.5.cloned.1.call-start
  45.9 2.1 %gather_fusion.1 = bf16[512,1024]{1,0:T(8,128)(2,1)S(1)} fusion(bf16[129,1024]{1,0:T(8,128)(2,1)S(1)} %concatenate.7, s32[1024]{0:T(1024)S(1)} %pad_clamp_fusion.1), kind=kCustom, calls=%fused_computation.1 | custom fusion | bytes 2099200 | tf_op jit(solution)/shard_map/gather | solution.py:34
  48.0 0.0 copy-start.5
  48.0 29.6 %all_to_all.57 = bf16[16,32,1024]{2,1,0:T(8,128)(2,1)} all-to-all(bf16[16,32,1024]{2,1,0:T(8,128)(2,1)S(1)} %bitcast.45), channel_id=1, replica_groups=mesh['ep'=16,'tp'=2] {'ep'}, dimensions={0} | all-to-all | bytes 2097152 | tf_op jit(solution)/shard_map/all_to_all | solution.py:37
  77.6 0.0 all-gather.5.cloned.1.call-update
  77.7 0.0 reduce-scatter.2.cloned.1.call-start
  77.7 0.0 copy-done.5
  77.7 0.1 copy.33
  77.9 0.1 reshape.125
  78.0 2.2 %scatter_custom_fusion = bf16[512]{0:T(512)(128)(2,1)S(1)} fusion(s32[256]{0:T(256)S(1)} %bitcast.57, bf16[256]{0:T(256)(128)(2,1)S(1)} %reshape.125, bf16[]{:T(256)} %constant.13.clone.1), kind=kCustom, calls=%fused_computation.49 | custom fusion | bytes 1026 | tf_op jit(solution)/shard_map/scatter | solution.py:27
  80.2 0.1 all_to_all.49
  80.3 8.9 %all_to_all.58 = bf16[16,32,1]{1,2,0:T(2,128)(2,1)S(1)} all-to-all(bf16[16,32,1]{1,2,0:T(2,128)(2,1)S(1)} %all_to_all.49), channel_id=1, replica_groups=mesh['ep'=16,'tp'=2] {'ep'}, dimensions={0} | all-to-all | bytes 2048 | tf_op jit(solution)/shard_map/all_to_all | solution.py:39
  89.2 0.1 reshape.88
  89.3 2.9 %copy.35 = bf16[2,512,1024]{1,2,0:T(8,128)(2,1)S(1)} copy(bf16[2,512,1024]{2,1,0:T(8,128)(2,1)} %all-gather.3.cloned.1.call-done) | data formatting | bytes 4194304 | tf_op jit(solution)/shard_map/all_gather | solution.py:43
  92.2 0.0 copy-start.1
  92.2 20.4 %all-gather.5.cloned.1.call-done = bf16[512,2048]{1,0:T(8,128)(2,1)} async-done(((bf16[512,1024]{1,0:T(8,128)(2,1)}), bf16[512,2048]{1,0:T(8,128)(2,1)}) %all-gather.5.cloned.1.call-update) | async-done | bytes 2097168 | tf_op jit(solution)/shard_map/all_gather | solution.py:42
  112.6 0.0 copy-done
  112.6 2.5 %fusion.3 = f32[512,256]{0,1:T(8,128)S(1)} fusion(bf16[512,2048]{1,0:T(8,128)(2,1)} %all-gather.5.cloned.1.call-done, bf16[1,2048,256]{2,1,0:T(8,128)(2,1)S(1)} %copy-done), kind=kOutput, calls=%fused_computation.17 | convolution fusion | flops 536870912 | bytes 3670016 | tf_op jit(solution)/shard_map/dot_general | solution.py:49
  115.1 0.0 copy-done.2
  115.1 0.0 copy-done.6
  115.2 0.8 fusion.6
  115.9 0.0 copy-start.10
  115.9 0.0 copy-done.1
  115.9 0.6 copy-done.8
  116.6 0.9 multiply_reduce_fusion.3
  117.5 0.0 copy-done.9
  117.5 0.0 copy-done.10
  117.5 0.0 copy-start.3
  117.5 0.8 fusion.1
  118.3 2.1 %add_convert_fusion = bf16[512,2048]{1,0:T(8,128)(2,1)} fusion(f32[512,2048]{1,0:T(8,128)S(1)} %fusion.1, bf16[512,256]{0,1:T(8,128)(2,1)S(1)} %get-tuple-element.45, bf16[1,2048,256]{2,1,0:T(8,128)(2,1)S(1)} %copy-done.2), kind=kOutput, calls=%fused_computation.6 | convolution fusion | flops 538968064 | bytes 7602176 | tf_op jit(solution)/shard_map/dot_general | solution.py:76
  120.4 0.0 reduce-scatter.2.cloned.1.call-update
  120.4 0.0 copy-start.4
  120.4 0.0 copy-start.7
  120.4 2.5 %multiply_reduce_fusion.2 = (f32[2048]{0:T(1024)S(1)}, bf16[2048,256]{0,1:T(8,128)(2,1)S(1)}) fusion(bf16[512,256]{0,1:T(8,128)(2,1)S(1)} %get-tuple-element.44, bf16[512,2048]{1,0:T(8,128)(2,1)} %all-gather.5.cloned.1.call-done), kind=kOutput, calls=%fused_computation.12 | convolution fusion | flops 538966016 | bytes 3416064 | tf_op jit(solution)/shard_map/dot_general | solution.py:67
  122.9 1.7 multiply_reduce_fusion.1
  124.6 6.5 %all-reduce.2 = (bf16[512]{0:T(512)(128)(2,1)S(1)}, f32[1,2048]{1,0:T(1,128)}, f32[1,2048]{1,0:T(1,128)}) all-reduce(f32[512]{0:T(512)S(1)} %get-tuple-element.43, f32[1,2048]{1,0:T(1,128)S(1)} %bitcast.54, f32[1,2048]{1,0:T(1,128)S(1)} %bitcast.55), channel_id=1, replica_groups=mesh['ep'=16,'tp'=2] {'tp'}, use_global_device_ids=true, to_apply=%region_6.7 | all-reduce | flops 4608 | bytes 35840 | tf_op jit(solution)/shard_map/psum | solution.py:85
  131.1 0.1 all_to_all.50
  131.2 13.0 %all_to_all.59 = bf16[16,32,1]{1,2,0:T(2,128)(2,1)S(1)} all-to-all(bf16[16,32,1]{1,2,0:T(2,128)(2,1)S(1)} %all_to_all.50), channel_id=1, replica_groups=mesh['ep'=16,'tp'=2] {'ep'}, dimensions={0} | all-to-all | bytes 2048 | tf_op jit(solution)/shard_map/all_to_all | solution.py:88
  144.2 8.7 %reduce-scatter.2.cloned.1.call-done = bf16[512,1024]{1,0:T(8,128)(2,1)} async-done(((bf16[512,2048]{1,0:T(8,128)(2,1)}), bf16[512,1024]{1,0:T(8,128)(2,1)}) %reduce-scatter.2.cloned.1.call-update) | async-done | bytes 1048592 | tf_op jit(solution)/shard_map/reduce_scatter | solution.py:79
  152.9 6.5 %all-to-all-start.3 = ((bf16[16,32,1024]{2,1,0:T(8,128)(2,1)}), bf16[16,32,1024]{2,1,0:T(8,128)(2,1)S(1)}, u32[]{:S(2)}, u32[]{:S(2)}) async-start(bf16[16,32,1024]{2,1,0:T(8,128)(2,1)} %bitcast.51), calls=%async_computation.4 | async-start | bytes 2097152 | tf_op jit(solution)/shard_map/all_to_all | solution.py:87
  159.4 2.3 %copy.39 = bf16[1,2048,256]{2,1,0:T(8,128)(2,1)} copy(bf16[1,2048,256]{1,2,0:T(8,128)(2,1)} %bitcast.53) | data formatting | bytes 2097152
  161.7 1.3 copy.38
  163.0 4.2 %multiply_reduce_fusion = (f32[256]{0:T(256)}, bf16[256,2048]{1,0:T(8,128)(2,1)}) fusion(bf16[512,2048]{0,1:T(8,128)(2,1)} %bitcast.50, f32[512]{0:T(512)S(1)} %reshape.88, f32[512,256]{0,1:T(8,128)} %copy-done.10, f32[512,256]{0,1:T(8,128)} %copy-done.9), kind=kOutput, calls=%fused_computation.10 | convolution fusion | flops 539885312 | bytes 4197376 | tf_op jit(solution)/shard_map/dot_general | solution.py:64
  167.2 0.1 all_to_all.48
  167.3 1.9 gather_fusion.3
  169.2 0.2 reshape.87
  169.4 0.6 copy.37
  170.0 14.3 %all-to-all-done.3 = bf16[16,32,1024]{2,1,0:T(8,128)(2,1)S(1)} async-done(((bf16[16,32,1024]{2,1,0:T(8,128)(2,1)}), bf16[16,32,1024]{2,1,0:T(8,128)(2,1)S(1)}, u32[]{:S(2)}, u32[]{:S(2)}) %all-to-all-start.3) | async-done | bytes 1048608 | tf_op jit(solution)/shard_map/all_to_all | solution.py:87
  184.3 1.2 gather_fusion.2
  185.5 0.2 gather.17
  185.7 2.1 %reduce_sum.58 = bf16[128,1024]{1,0:T(8,128)(2,1)} reduce(bf16[128,2,1024]{2,1,0:T(2,128)(2,1)S(1)} %gather.17, bf16[]{:T(256)} %constant.13.clone.1), dimensions={1}, to_apply=%region_4.5 | reduce | flops 131072 | bytes 786434 | tf_op jit(solution)/shard_map/reduce_sum | solution.py:93
  (18 shorter events, 0.1 us)
Async XLA Ops:
  7.2 105.4 %copy-start = (bf16[1,2048,256]{2,1,0:T(8,128)(2,1)S(1)}, bf16[1,2048,256]{2,1,0:T(8,128)(2,1)}, u32[]{:S(2)}) copy-start(bf16[1,2048,256]{2,1,0:T(8,128)(2,1)} %param.11) | copy-start | bytes 3145732
  7.2 82.1 %all-gather.3.cloned.1.call-start = ((), (), s32[]{:S(2)}) async-start(), calls=%async_computation.6 | async-start | bytes 3145728 | tf_op jit(solution)/shard_map/all_gather | solution.py:43
  45.9 66.7 %all-gather.5.cloned.1.call-start = ((), (), s32[]{:S(2)}) async-start(), calls=%async_computation.7 | async-start | bytes 3145728 | tf_op jit(solution)/shard_map/all_gather | solution.py:42
  48.0 29.7 %copy-start.5 = (bf16[128,2]{0,1:T(2,128)(2,1)S(1)}, bf16[128,2]{0,1:T(2,128)(2,1)}, u32[]{:S(2)}) copy-start(bf16[128,2]{0,1:T(2,128)(2,1)} %param.9) | copy-start | bytes 1540
  77.7 75.2 %reduce-scatter.2.cloned.1.call-start = ((), (), s32[]{:S(2)}) async-start(), calls=%async_computation.8 | async-start | bytes 3145728 | tf_op jit(solution)/shard_map/reduce_scatter | solution.py:79
  92.2 23.7 %copy-start.1 = (bf16[2,512,1024]{1,2,0:T(8,128)(2,1)}, bf16[2,512,1024]{1,2,0:T(8,128)(2,1)S(1)}, u32[]{:S(2)}) copy-start(bf16[2,512,1024]{1,2,0:T(8,128)(2,1)S(1)} %copy.35) | copy-start | bytes 6291460
  112.6 2.5 %copy-start.2 = (bf16[1,2048,256]{2,1,0:T(8,128)(2,1)S(1)}, bf16[1,2048,256]{2,1,0:T(8,128)(2,1)}, u32[]{:S(2)}) copy-start(bf16[1,2048,256]{2,1,0:T(8,128)(2,1)} %param.12) | copy-start | bytes 3145732
  112.6 2.5 %copy-start.6 = (bf16[512,2048]{1,0:T(8,128)(2,1)S(1)}, bf16[512,2048]{1,0:T(8,128)(2,1)}, u32[]{:S(2)}) copy-start(bf16[512,2048]{1,0:T(8,128)(2,1)} %all-gather.5.cloned.1.call-done) | copy-start | bytes 6291460
  115.2 2.3 %copy-start.9 = (f32[512,256]{0,1:T(8,128)}, f32[512,256]{0,1:T(8,128)S(1)}, u32[]{:S(2)}) copy-start(f32[512,256]{0,1:T(8,128)S(1)} %fusion.3) | copy-start | bytes 1572868
  115.2 1.4 copy-start.8
  115.9 1.6 copy-start.10
  117.5 0.8 copy-start.3
  120.4 2.5 %copy-start.4 = (bf16[512,256]{0,1:T(8,128)(2,1)S(1)}, bf16[512,256]{0,1:T(8,128)(2,1)}, u32[]{:S(2)}) copy-start(bf16[512,256]{0,1:T(8,128)(2,1)} %copy-done.3) | copy-start | bytes 786436
  120.4 2.5 %copy-start.7 = (bf16[512,2048]{1,0:T(8,128)(2,1)S(1)}, bf16[512,2048]{1,0:T(8,128)(2,1)}, u32[]{:S(2)}) copy-start(bf16[512,2048]{1,0:T(8,128)(2,1)} %all-gather.5.cloned.1.call-done) | copy-start | bytes 6291460
  152.9 31.4 %all-to-all-start.3 = ((bf16[16,32,1024]{2,1,0:T(8,128)(2,1)}), bf16[16,32,1024]{2,1,0:T(8,128)(2,1)S(1)}, u32[]{:S(2)}, u32[]{:S(2)}) async-start(bf16[16,32,1024]{2,1,0:T(8,128)(2,1)} %bitcast.51), calls=%async_computation.4 | async-start | bytes 2097152 | tf_op jit(solution)/shard_map/all_to_all | solution.py:87
Sparse Core Ops, SparseCore 0:
  46.0 31.9 all-gather.2
  79.5 33.0 all-gather.4
  120.5 32.2 reduce-scatter.1
